TPU v7x, 32 devices: a whole 2x2x4 slice. The times are simulated.
32 devices in a mesh: gr: 2 (over x), fs: 8 (over z, y), tp: 2 (over core).
Axes of the slice: x: 2, y: 2, z: 4, core: 2. Of those that a mesh axis runs over, the one named last changes fastest.
Arguments:
- tokens: bfloat16 [4, 2048, 2048], P(('gr', 'tp')), may hold values from -6 to 6
- gate_master: float32 [3, 2048, 7168], P(None, 'fs', ('gr', 'tp')), may hold values from -0.125 to 0.125
- up_master: float32 [3, 2048, 7168], P(None, 'fs', ('gr', 'tp')), may hold values from -0.125 to 0.125
- down_master: float32 [3, 7168, 2048], P(None, 'fs', ('gr', 'tp')), may hold values from -0.0625 to 0.0625
- norm_gain: float32 [2048], P('fs'), may hold values from 0.1 to 1.9
- route: int32 [4, 2048, 2], P(('gr', 'tp')), may hold values from 0 to 2, all different within a row
- route_weight: float32 [4, 2048, 2], P(('gr', 'tp')), may hold values from 0.05 to 1
Outputs:
- gate_out: bfloat16 [3, 2048, 7168], P(None, None, 'fs')
- up_out: bfloat16 [3, 2048, 7168], P(None, None, 'fs')
- down_out: bfloat16 [3, 7168, 2048], P(None, 'fs')
- mixed: bfloat16 [4, 2048, 2048], P(('gr', 'tp'), 'fs')
Inputs may be any that keep to these rules, and one draw needn't show every extreme that they name: `route`: each token names two different experts; every expert is named by some token.
All inputs are finite; a program needn't handle non-finite values.
Results may differ from a plain program's by a relative error of at most 0.024.
Values may be sent and summed in bfloat16 or wider, within the bound.
A program may use at most 192 MiB of HBM per device.

v0:
```python
import jax
import jax.numpy as jnp
from jax import lax
from jax.sharding import PartitionSpec as P


def normalize(rows_in):
    values = rows_in.astype(jnp.float32)
    scaled = values * lax.rsqrt(jnp.mean(values * values, axis=-1, keepdims=True) + 1e-06)
    return scaled.astype(jnp.bfloat16)


def mixing(chosen, weights, experts):
    share = weights / jnp.sum(weights, axis=-1, keepdims=True)
    labels = jnp.arange(experts, dtype=jnp.int32)
    match = (chosen[:, :, None] == labels[None, None, :]).astype(jnp.float32)
    return jnp.sum(share[:, :, None] * match, axis=1)


def expert_term(normed, mix_column, gate_weight, up_weight, down_weight):
    gate_act = jnp.dot(normed, gate_weight, preferred_element_type=jnp.float32)
    up_act = jnp.dot(normed, up_weight, preferred_element_type=jnp.float32)
    hidden = (jax.nn.silu(gate_act) * up_act).astype(jnp.bfloat16)
    projected = jnp.dot(hidden, down_weight, preferred_element_type=jnp.float32)
    return mix_column * projected


def shards(tokens, gate_master, up_master, down_master, norm_gain, route, route_weight):
    scaled_gain = norm_gain[None, :, None]
    gate_local = (scaled_gain * gate_master).astype(jnp.bfloat16)
    up_local = (scaled_gain * up_master).astype(jnp.bfloat16)
    down_local = down_master.astype(jnp.bfloat16)
    experts = gate_local.shape[0]
    normed = normalize(tokens[0])
    combine = mixing(route[0], route_weight[0], experts)
    width = normed.shape[1]
    gate_list = []
    up_list = []
    down_list = []
    total = jnp.zeros((normed.shape[0], width), jnp.float32)
    for index in range(experts):
        gate_rows, up_rows, down_full = (
            lax.all_gather(gate_local[index], ("gr", "tp"), axis=1, tiled=True),
            lax.all_gather(up_local[index], ("gr", "tp"), axis=1, tiled=True),
            lax.all_gather(down_local[index], ("gr", "tp"), axis=1, tiled=True),
        )
        gate_block, up_block = (
            lax.all_to_all(gate_rows, "fs", split_axis=1, concat_axis=0, tiled=True),
            lax.all_to_all(up_rows, "fs", split_axis=1, concat_axis=0, tiled=True),
        )
        total = total + expert_term(
            normed, combine[:, index : index + 1], gate_block, up_block, down_full
        )
        gate_list.append(gate_block)
        up_list.append(up_block)
        down_list.append(down_full)
    gate_out = jnp.stack(gate_list, axis=0)
    up_out = jnp.stack(up_list, axis=0)
    down_out = jnp.stack(down_list, axis=0)
    summed = lax.psum_scatter(total.astype(jnp.bfloat16), "fs", scatter_dimension=0, tiled=True)
    mixed = summed[None]
    return (gate_out, up_out, down_out, mixed)


def solution(mesh):
    in_specs = (
        P(("gr", "tp"), None, None),
        P(None, "fs", ("gr", "tp")),
        P(None, "fs", ("gr", "tp")),
        P(None, "fs", ("gr", "tp")),
        P("fs"),
        P(("gr", "tp"), None, None),
        P(("gr", "tp"), None, None),
    )
    out_specs = (
        P(None, None, "fs"),
        P(None, None, "fs"),
        P(None, "fs", None),
        P(("gr", "tp"), "fs", None),
    )
    return jax.shard_map(shards, mesh=mesh, in_specs=in_specs, out_specs=out_specs, check_vma=False)
```

profile of v0, /device:TPU:0, one launch (start us, length us, event | category | flops | bytes accessed | tf_op | source)
XLA Modules:
  0.0 764.3 jit_solution(10125969847166633548)
XLA Ops:
  7.2 5.2 multiply_convert_fusion.3
  12.4 1.6 fusion.29
  14.1 1.6 fusion.28
  15.7 0.7 all-gather.19.cloned.1.call-update
  16.5 0.5 all-gather.25.cloned.1.call-update
  17.0 31.4 %all-gather.21.cloned.1.call-done = bf16[1,256,7168]{2,1,0:T(8,128)(2,1)} async-done(((bf16[1,256,1792]{2,1,0:T(8,128)(2,1)}), bf16[1,256,7168]{2,1,0:T(8,128)(2,1)}) %all-gather.21.cloned.1.call-update) | async-done | bytes 3670032 | tf_op jit(solution)/shard_map/all_gather | solution.py:43
  48.4 2.8 copy.34
  51.2 2.4 copy.28
  53.6 5.5 all-to-all-start.1
  59.2 0.5 all-gather.23.cloned.1.call-update
  59.7 22.3 %all-gather.27.cloned.1.call-done = bf16[1,256,7168]{2,1,0:T(8,128)(2,1)} async-done(((bf16[1,256,1792]{2,1,0:T(8,128)(2,1)}), bf16[1,256,7168]{2,1,0:T(8,128)(2,1)}) %all-gather.27.cloned.1.call-update) | async-done | bytes 3670032 | tf_op jit(solution)/shard_map/all_gather | solution.py:44
  82.0 2.8 copy.37
  84.8 2.4 copy.31
  87.3 54.3 %all-to-all-done.1 = bf16[256,8,896]{2,0,1:T(8,128)(2,1)} async-done(((bf16[256,8,896]{2,0,1:T(8,128)(2,1)}), bf16[256,8,896]{2,0,1:T(8,128)(2,1)}, u32[]{:S(2)}, u32[]{:S(2)}) %all-to-all-start.1) | async-done | bytes 3670048 | tf_op jit(solution)/shard_map/all_to_all | solution.py:48
  141.6 4.5 all-to-all-start.4
  146.2 0.5 all-gather.29.cloned.1.call-update
  146.7 2.8 copy.33
  149.5 2.4 copy.27
  151.9 75.7 %all-to-all-done.4 = bf16[256,8,896]{2,0,1:T(8,128)(2,1)} async-done(((bf16[256,8,896]{2,0,1:T(8,128)(2,1)}), bf16[256,8,896]{2,0,1:T(8,128)(2,1)}, u32[]{:S(2)}, u32[]{:S(2)}) %all-to-all-start.4) | async-done | bytes 3670048 | tf_op jit(solution)/shard_map/all_to_all | solution.py:49
  227.6 4.5 all-to-all-start
  232.2 2.9 convert_element_type.45
  235.1 1.6 fusion.27
  236.8 0.7 all-gather.31.cloned.1.call-update
  237.5 2.8 copy.36
  240.3 2.4 copy.30
  242.7 70.7 %all-to-all-done = bf16[256,8,896]{2,0,1:T(8,128)(2,1)} async-done(((bf16[256,8,896]{2,0,1:T(8,128)(2,1)}), bf16[256,8,896]{2,0,1:T(8,128)(2,1)}, u32[]{:S(2)}, u32[]{:S(2)}) %all-to-all-start) | async-done | bytes 3670048 | tf_op jit(solution)/shard_map/all_to_all | solution.py:48
  313.5 4.5 all-to-all-start.3
  318.0 0.7 all-gather.35.cloned.1.call-update
  318.9 5.1 fusion
  324.0 2.8 copy.35
  326.8 2.4 copy.29
  329.2 70.1 %all-to-all-done.3 = bf16[256,8,896]{2,0,1:T(8,128)(2,1)} async-done(((bf16[256,8,896]{2,0,1:T(8,128)(2,1)}), bf16[256,8,896]{2,0,1:T(8,128)(2,1)}, u32[]{:S(2)}, u32[]{:S(2)}) %all-to-all-start.3) | async-done | bytes 3670048 | tf_op jit(solution)/shard_map/all_to_all | solution.py:49
  399.3 16.6 %all-to-all-start.2 = ((bf16[256,8,896]{2,0,1:T(8,128)(2,1)}), bf16[256,8,896]{2,0,1:T(8,128)(2,1)}, u32[]{:S(2)}, u32[]{:S(2)}) async-start(bf16[256,8,896]{2,0,1:T(8,128)(2,1)} %copy.29), calls=%async_computation.2 | async-start | bytes 7340032 | tf_op jit(solution)/shard_map/all_to_all | solution.py:48
  416.0 2.8 copy.38
  418.8 2.4 copy.32
  421.2 14.2 %fusion.21 = f32[2048,896]{1,0:T(8,128)} fusion(bf16[2048,896]{1,0:T(8,128)(2,1)} %bitcast.20, bf16[1,2048,2048]{2,1,0:T(8,128)(2,1)} %param.7, f32[2048]{0:T(1024)S(1)} %add_rsqrt_fusion), kind=kOutput, calls=%fused_computation.30 | convolution fusion | flops 7528775680 | bytes 19406848 | tf_op jit(solution)/shard_map/dot_general | solution.py:21
  435.5 26.7 %fusion.3 = f32[2048,2048]{1,0:T(8,128)} fusion(f32[2048,896]{1,0:T(8,128)} %fusion.21, bf16[2048,896]{1,0:T(8,128)(2,1)} %bitcast.21, bf16[1,896,2048]{2,1,0:T(8,128)(2,1)} %all-gather.33.cloned.1.call-done, bf16[1,2048,2048]{2,1,0:T(8,128)(2,1)} %param.7, f32[2048]{0:T(1024)S(1)} %add_rsqrt_fusion), kind=kOutput, calls=%fused_computation.14 | convolution fusion | flops 15055978496 | bytes 39854080 | tf_op jit(solution)/shard_map/dot_general | solution.py:24
  462.2 35.0 %all-to-all-done.2 = bf16[256,8,896]{2,0,1:T(8,128)(2,1)} async-done(((bf16[256,8,896]{2,0,1:T(8,128)(2,1)}), bf16[256,8,896]{2,0,1:T(8,128)(2,1)}, u32[]{:S(2)}, u32[]{:S(2)}) %all-to-all-start.2) | async-done | bytes 3670048 | tf_op jit(solution)/shard_map/all_to_all | solution.py:48
  497.2 4.5 all-to-all-start.5
  501.8 14.2 %fusion.25 = f32[2048,896]{1,0:T(8,128)} fusion(bf16[2048,896]{1,0:T(8,128)(2,1)} %bitcast.16, bf16[1,2048,2048]{2,1,0:T(8,128)(2,1)} %param.7, f32[2048]{0:T(1024)S(1)} %add_rsqrt_fusion), kind=kOutput, calls=%fused_computation.31 | convolution fusion | flops 7528775680 | bytes 19406848 | tf_op jit(solution)/shard_map/dot_general | solution.py:21
  516.0 14.2 %fusion.17 = f32[2048,896]{1,0:T(8,128)} fusion(bf16[2048,896]{1,0:T(8,128)(2,1)} %bitcast.24, bf16[1,2048,2048]{2,1,0:T(8,128)(2,1)} %param.7, f32[2048]{0:T(1024)S(1)} %add_rsqrt_fusion), kind=kOutput, calls=%fused_computation.29 | convolution fusion | flops 7528775680 | bytes 19406848 | tf_op jit(solution)/shard_map/dot_general | solution.py:21
  530.2 26.9 %fusion.4 = f32[2048,2048]{1,0:T(8,128)} fusion(f32[2048,896]{1,0:T(8,128)} %fusion.25, bf16[2048,896]{1,0:T(8,128)(2,1)} %bitcast.17, bf16[1,896,2048]{2,1,0:T(8,128)(2,1)} %all-gather.31.cloned.1.call-done, bf16[1,2048,2048]{2,1,0:T(8,128)(2,1)} %param.7, f32[2048]{0:T(1024)S(1)} %add_rsqrt_fusion), kind=kOutput, calls=%fused_computation.15 | convolution fusion | flops 15055978496 | bytes 39854080 | tf_op jit(solution)/shard_map/dot_general | solution.py:24
  557.1 25.8 %all-to-all-done.5 = bf16[256,8,896]{2,0,1:T(8,128)(2,1)} async-done(((bf16[256,8,896]{2,0,1:T(8,128)(2,1)}), bf16[256,8,896]{2,0,1:T(8,128)(2,1)}, u32[]{:S(2)}, u32[]{:S(2)}) %all-to-all-start.5) | async-done | bytes 3670048 | tf_op jit(solution)/shard_map/all_to_all | solution.py:49
  582.9 28.4 %add_convert_fusion = bf16[2048,2048]{1,0:T(8,128)(2,1)} fusion(f32[2048,2048]{1,0:T(8,128)} %fusion.3, f32[2048,2048]{1,0:T(8,128)} %fusion.4, f32[2048]{0:T(1024)S(1)} %bitcast.95, f32[2048]{0:T(1024)S(1)} %bitcast.96, f32[2048]{0:T(1024)S(1)} %bitcast.94, f32[2048,896]{1,0:T(8,128)} %fusion.17, bf16[2048,896]{1,0:T(8,128)(2,1)} %bitcast.25, ...), kind=kOutput, calls=%fused_computation.4 | convolution fusion | flops 15081144320 | bytes 65044480 | tf_op jit(solution)/shard_map/dot_general | solution.py:24
  611.3 9.8 %pad_maximum_fusion.2 = bf16[3,896,2048]{2,1,0:T(8,128)(2,1)} fusion(bf16[1,896,2048]{2,1,0:T(8,128)(2,1)} %all-gather.35.cloned.1.call-done, bf16[1,896,2048]{2,1,0:T(8,128)(2,1)} %all-gather.33.cloned.1.call-done, bf16[1,896,2048]{2,1,0:T(8,128)(2,1)} %all-gather.31.cloned.1.call-done), kind=kLoop, calls=%fused_computation.7 | loop fusion | flops 11010048 | bytes 22020096 | tf_op jit(solution)/shard_map/stack | solution.py:59
  621.1 9.8 %pad_maximum_fusion.1 = bf16[3,2048,896]{2,1,0:T(8,128)(2,1)} fusion(bf16[1,2048,896]{2,1,0:T(8,128)(2,1)} %bitcast.11, bf16[1,2048,896]{2,1,0:T(8,128)(2,1)} %bitcast.9, bf16[1,2048,896]{2,1,0:T(8,128)(2,1)} %bitcast.7), kind=kLoop, calls=%fused_computation.6 | loop fusion | flops 11010048 | bytes 22020096 | tf_op jit(solution)/shard_map/stack | solution.py:58
  630.9 9.8 %pad_maximum_fusion = bf16[3,2048,896]{2,1,0:T(8,128)(2,1)} fusion(bf16[1,2048,896]{2,1,0:T(8,128)(2,1)} %bitcast.5, bf16[1,2048,896]{2,1,0:T(8,128)(2,1)} %bitcast.3, bf16[1,2048,896]{2,1,0:T(8,128)(2,1)} %bitcast.1), kind=kLoop, calls=%fused_computation.5 | loop fusion | flops 11010048 | bytes 22020096 | tf_op jit(solution)/shard_map/stack | solution.py:57
  640.6 116.5 %reduce-scatter.2.cloned.1.call-done = bf16[256,2048]{1,0:T(8,128)(2,1)} async-done(((bf16[2048,2048]{1,0:T(8,128)(2,1)}), bf16[256,2048]{1,0:T(8,128)(2,1)}) %reduce-scatter.2.cloned.1.call-update) | async-done | bytes 1048592 | tf_op jit(solution)/shard_map/reduce_scatter | solution.py:60
  (30 shorter events, 0.7 us)
Async XLA Ops:
  7.2 41.2 %all-gather.21.cloned.1.call-start = ((), (), s32[]{:S(2)}) async-start(), calls=%async_computation.9 | async-start | bytes 4587520 | tf_op jit(solution)/shard_map/all_gather | solution.py:43
  14.0 68.0 %all-gather.27.cloned.1.call-start = ((), (), s32[]{:S(2)}) async-start(), calls=%async_computation.12 | async-start | bytes 4587520 | tf_op jit(solution)/shard_map/all_gather | solution.py:44
  15.7 131.0 %all-gather.19.cloned.1.call-start = ((), (), s32[]{:S(2)}) async-start(), calls=%async_computation.8 | async-start | bytes 4587520 | tf_op jit(solution)/shard_map/all_gather | solution.py:43
  16.4 221.1 %all-gather.25.cloned.1.call-start = ((), (), s32[]{:S(2)}) async-start(), calls=%async_computation.11 | async-start | bytes 4587520 | tf_op jit(solution)/shard_map/all_gather | solution.py:44
  53.6 88.0 %all-to-all-start.1 = ((bf16[256,8,896]{2,0,1:T(8,128)(2,1)}), bf16[256,8,896]{2,0,1:T(8,128)(2,1)}, u32[]{:S(2)}, u32[]{:S(2)}) async-start(bf16[256,8,896]{2,0,1:T(8,128)(2,1)} %copy.28), calls=%async_computation.1 | async-start | bytes 7340032 | tf_op jit(solution)/shard_map/all_to_all | solution.py:48
  59.1 264.9 %all-gather.23.cloned.1.call-start = ((), (), s32[]{:S(2)}) async-start(), calls=%async_computation.10 | async-start | bytes 4587520 | tf_op jit(solution)/shard_map/all_gather | solution.py:43
  141.6 86.0 %all-to-all-start.4 = ((bf16[256,8,896]{2,0,1:T(8,128)(2,1)}), bf16[256,8,896]{2,0,1:T(8,128)(2,1)}, u32[]{:S(2)}, u32[]{:S(2)}) async-start(bf16[256,8,896]{2,0,1:T(8,128)(2,1)} %copy.31), calls=%async_computation.4 | async-start | bytes 7340032 | tf_op jit(solution)/shard_map/all_to_all | solution.py:49
  146.1 269.9 %all-gather.29.cloned.1.call-start = ((), (), s32[]{:S(2)}) async-start(), calls=%async_computation.13 | async-start | bytes 4587520 | tf_op jit(solution)/shard_map/all_gather | solution.py:44
  227.6 85.9 %all-to-all-start = ((bf16[256,8,896]{2,0,1:T(8,128)(2,1)}), bf16[256,8,896]{2,0,1:T(8,128)(2,1)}, u32[]{:S(2)}, u32[]{:S(2)}) async-start(bf16[256,8,896]{2,0,1:T(8,128)(2,1)} %copy.27), calls=%async_computation | async-start | bytes 7340032 | tf_op jit(solution)/shard_map/all_to_all | solution.py:48
  232.1 203.3 %all-gather.33.cloned.1.call-start = ((), (), s32[]{:S(2)}) async-start(), calls=%async_computation.15 | async-start | bytes 4587520 | tf_op jit(solution)/shard_map/all_gather | solution.py:45
  236.7 293.5 %all-gather.31.cloned.1.call-start = ((), (), s32[]{:S(2)}) async-start(), calls=%async_computation.14 | async-start | bytes 4587520 | tf_op jit(solution)/shard_map/all_gather | solution.py:45
  240.3 78.5 %copy-start = (f32[1,2048,2]{1,2,0:T(2,128)S(1)}, f32[1,2048,2]{1,2,0:T(2,128)}, u32[]{:S(2)}) copy-start(f32[1,2048,2]{1,2,0:T(2,128)} %param.13) | copy-start | bytes 49156
  240.3 78.5 %copy-start.1 = (s32[1,2048,2]{1,2,0:T(2,128)S(1)}, s32[1,2048,2]{1,2,0:T(2,128)}, u32[]{:S(2)}) copy-start(s32[1,2048,2]{1,2,0:T(2,128)} %param.12) | copy-start | bytes 49156
  313.5 85.9 %all-to-all-start.3 = ((bf16[256,8,896]{2,0,1:T(8,128)(2,1)}), bf16[256,8,896]{2,0,1:T(8,128)(2,1)}, u32[]{:S(2)}, u32[]{:S(2)}) async-start(bf16[256,8,896]{2,0,1:T(8,128)(2,1)} %copy.30), calls=%async_computation.3 | async-start | bytes 7340032 | tf_op jit(solution)/shard_map/all_to_all | solution.py:49
  318.0 239.1 %all-gather.35.cloned.1.call-start = ((), (), s32[]{:S(2)}) async-start(), calls=%async_computation.16 | async-start | bytes 4587520 | tf_op jit(solution)/shard_map/all_gather | solution.py:45
  399.3 97.9 %all-to-all-start.2 = ((bf16[256,8,896]{2,0,1:T(8,128)(2,1)}), bf16[256,8,896]{2,0,1:T(8,128)(2,1)}, u32[]{:S(2)}, u32[]{:S(2)}) async-start(bf16[256,8,896]{2,0,1:T(8,128)(2,1)} %copy.29), calls=%async_computation.2 | async-start | bytes 7340032 | tf_op jit(solution)/shard_map/all_to_all | solution.py:48
  497.2 85.7 %all-to-all-start.5 = ((bf16[256,8,896]{2,0,1:T(8,128)(2,1)}), bf16[256,8,896]{2,0,1:T(8,128)(2,1)}, u32[]{:S(2)}, u32[]{:S(2)}) async-start(bf16[256,8,896]{2,0,1:T(8,128)(2,1)} %copy.32), calls=%async_computation.5 | async-start | bytes 7340032 | tf_op jit(solution)/shard_map/all_to_all | solution.py:49
  501.7 255.4 %reduce-scatter.2.cloned.1.call-start = ((), (), s32[]{:S(2)}) async-start(), calls=%async_computation.7 | async-start | bytes 9437184 | tf_op jit(solution)/shard_map/reduce_scatter | solution.py:60
Sparse Core Ops, SparseCore 0:
  14.1 34.1 all-gather.20
  50.5 31.4 all-gather.26
  84.2 31.4 all-gather.18
  117.7 31.4 all-gather.24
  150.6 31.4 all-gather.22
  183.5 31.4 all-gather.28
  236.8 31.8 all-gather.32
  270.8 31.4 all-gather.30
  320.4 31.8 all-gather.34
  611.5 145.5 reduce-scatter.1
where the time goes:
time: 773 us; the launch traced here: 764 us
  waiting for transfers between devices  506 us (65%)
  matrix products  125 us (16%)
  other arithmetic  42.6 us (6%)
  starting transfers between devices  40.6 us (5%)
  local copies, waits for them, and re-layouts  36.1 us (5%)
  between operations  14.8 us (2%)
    all_to_all x3, waiting for transfers between devices, shards(): lax.all_to_all(up_rows, 'fs', split_axis=1, concat_axis=0, tiled=True)  172 us
    all_to_all x3, waiting for transfers between devices, shards(): lax.all_to_all(gate_rows, 'fs', split_axis=1, concat_axis=0, tiled=True)  160 us
    reduce_scatter x1, waiting for transfers between devices, shards(): lax.psum_scatter(total.astype(jnp.bfloat16), 'fs', scatter_dimension=0, t...  116 us
    dot_general x3, matrix products, expert_term(): projected = jnp.dot(hidden, down_weight, preferred_element_type=jnp.float32)  82 us
    dot_general x3, matrix products, expert_term(): gate_act = jnp.dot(normed, gate_weight, preferred_element_type=jnp.float32)  42.7 us
    all_gather x3, waiting for transfers between devices, shards(): lax.all_gather(gate_local[index], ('gr', 'tp'), axis=1, tiled=True)  31.4 us
    all_to_all x3, starting transfers between devices, shards(): lax.all_to_all(gate_rows, 'fs', split_axis=1, concat_axis=0, tiled=True)  26.6 us
    all_gather x3, waiting for transfers between devices, shards(): lax.all_gather(up_local[index], ('gr', 'tp'), axis=1, tiled=True)  22.4 us
  transfers between devices with their start and end apart: 16, of which 9 were waited for; matrix products, arithmetic and copies ran while one was open for 22% of the time, Pallas kernels for 0%

commit v1 on v0

--- a/solution.py
+++ b/solution.py
@@ -2,6 +2,24 @@
 import jax.numpy as jnp
 from jax import lax
 from jax.sharding import PartitionSpec as P
+
+
+def link_strips_all_all(incoming_x, at_axis, slab_in):
+    even = incoming_x.shape
+    prior = incoming_x.reshape(
+        *even[:at_axis], slab_in, even[at_axis] // slab_in, *even[at_axis + 1 :]
+    )
+    d_next = jnp.moveaxis(prior, at_axis, 0)
+    return d_next
+
+
+def pack_pipes_up(vals, out_dim):
+    vals = jnp.moveaxis(vals, 0, out_dim)
+    f_next = vals.shape
+    tile_out = vals.reshape(
+        *f_next[:out_dim], f_next[out_dim] * f_next[out_dim + 1], *f_next[out_dim + 2 :]
+    )
+    return tile_out
 
 
 def normalize(rows_in):
@@ -44,9 +62,26 @@
             lax.all_gather(up_local[index], ("gr", "tp"), axis=1, tiled=True),
             lax.all_gather(down_local[index], ("gr", "tp"), axis=1, tiled=True),
         )
+
+        def refer_things(obj, tile_in, inputs, row_axis):
+            known = lax.axis_index(row_axis)
+            seen_now = lax.axis_size(row_axis)
+            a_next, u_next = (seen_now, known)
+            e_now = link_strips_all_all(inputs, tile_in, a_next)
+            fields = [e_now[u_next]]
+            for ix in range(1, a_next):
+                fresh = e_now[u_next ^ ix]
+                extra = lax.ppermute(
+                    fresh, axis_name=row_axis, perm=[(idx, idx ^ ix) for idx in range(a_next)]
+                )
+                fields.append(extra)
+            e_now = jnp.stack(fields, axis=0)[u_next ^ jnp.arange(a_next)]
+            r1 = pack_pipes_up(e_now, obj)
+            return r1
+
         gate_block, up_block = (
             lax.all_to_all(gate_rows, "fs", split_axis=1, concat_axis=0, tiled=True),
-            lax.all_to_all(up_rows, "fs", split_axis=1, concat_axis=0, tiled=True),
+            refer_things(0, 1, up_rows, "fs"),
         )
         total = total + expert_term(
             normed, combine[:, index : index + 1], gate_block, up_block, down_full

time: 773 us -> 801 us (1.036)
  waiting for transfers between devices: 506 us -> 381 us
  local copies, waits for them, and re-layouts: 36.1 us -> 124 us
  starting transfers between devices: 40.6 us -> 110 us
    all_to_all x3 -> x0, waiting for transfers between devices: 172 us -> none  [shards(): lax.all_to_all(up_rows, 'fs', split_axis=1, concat_axis=0, tiled=True)]
    ppermute x0 -> x21, waiting for transfers between devices: none -> 116 us  [refer_things(): lax.ppermute(fresh, axis_name=row_axis, perm=[(idx, idx ^ ix) for idx in...]
    ppermute x0 -> x21, starting transfers between devices: none -> 79.8 us  [refer_things(): lax.ppermute(fresh, axis_name=row_axis, perm=[(idx, idx ^ ix) for idx in...]
    all_to_all x3, waiting for transfers between devices: 160 us -> 80.7 us  [shards(): lax.all_to_all(gate_rows, 'fs', split_axis=1, concat_axis=0, tiled=True)]
    another operation x0 -> x29, local copies, waits for them, and re-layouts: none -> 41.3 us
    unnamed x10 -> x45, local copies, waits for them, and re-layouts: 16.6 us -> 44.6 us
    all_gather x3, waiting for transfers between devices: 31.4 us -> 47.1 us  [shards(): lax.all_gather(gate_local[index], ('gr', 'tp'), axis=1, tiled=True)]
    gather x0 -> x3, local copies, waits for them, and re-layouts: none -> 14.7 us  [refer_things(): e_now = jnp.stack(fields, axis=0)[u_next ^ jnp.arange(a_next)]]
  transfers between devices with their start and end apart: 16 -> 34, of which waited for: 9 -> 13; matrix products, arithmetic and copies ran while one was open for 22% -> 30% of each run, Pallas kernels for 0% -> 0%
where the time goes in v1:
time: 801 us; the launch traced here: 794 us
  waiting for transfers between devices  381 us (48%)
  matrix products  125 us (16%)
  local copies, waits for them, and re-layouts  124 us (15%)
  starting transfers between devices  110 us (14%)
  other arithmetic  39.6 us (5%)
  between operations  14.6 us (2%)
    reduce_scatter x1, waiting for transfers between devices, shards(): lax.psum_scatter(total.astype(jnp.bfloat16), 'fs', scatter_dimension=0, t...  119 us
    ppermute x21, waiting for transfers between devices, refer_things(): lax.ppermute(fresh, axis_name=row_axis, perm=[(idx, idx ^ ix) for idx in...  116 us
    dot_general x3, matrix products, expert_term(): projected = jnp.dot(hidden, down_weight, preferred_element_type=jnp.float32)  82.6 us
    all_to_all x3, waiting for transfers between devices, shards(): lax.all_to_all(gate_rows, 'fs', split_axis=1, concat_axis=0, tiled=True)  80.7 us
    ppermute x21, starting transfers between devices, refer_things(): lax.ppermute(fresh, axis_name=row_axis, perm=[(idx, idx ^ ix) for idx in...  79.8 us
    all_gather x3, waiting for transfers between devices, shards(): lax.all_gather(gate_local[index], ('gr', 'tp'), axis=1, tiled=True)  47.1 us
    unnamed x45, local copies, waits for them, and re-layouts  44.6 us
    dot_general x3, matrix products, expert_term(): gate_act = jnp.dot(normed, gate_weight, preferred_element_type=jnp.float32)  42.7 us
  transfers between devices with their start and end apart: 34, of which 13 were waited for; matrix products, arithmetic and copies ran while one was open for 30% of the time, Pallas kernels for 0%

profile of v1, /device:TPU:0, one launch (start us, length us, event | category | flops | bytes accessed | tf_op | source)
XLA Modules:
  0.0 794.0 jit_solution(15671959436764205879)
XLA Ops:
  7.2 6.1 copy.83
  13.3 6.1 copy.87
  19.4 5.1 multiply_convert_fusion.3
  30.4 2.9 convert_element_type.45
  35.7 24.9 %all-gather.19.cloned.1.call-done = bf16[1,256,7168]{1,2,0:T(8,128)(2,1)} async-done(((bf16[1,256,1792]{1,2,0:T(8,128)(2,1)}), bf16[1,256,7168]{1,2,0:T(8,128)(2,1)}) %all-gather.19.cloned.1.call-update) | async-done | bytes 3670032 | tf_op jit(solution)/shard_map/all_gather | solution.py:61
  60.5 6.2 copy.84
  66.7 5.6 all-to-all-start
  73.3 5.1 fusion
  78.5 15.7 %all-gather.21.cloned.1.call-done = bf16[1,256,7168]{1,2,0:T(8,128)(2,1)} async-done(((bf16[1,256,1792]{1,2,0:T(8,128)(2,1)}), bf16[1,256,7168]{1,2,0:T(8,128)(2,1)}) %all-gather.21.cloned.1.call-update) | async-done | bytes 3670032 | tf_op jit(solution)/shard_map/all_gather | solution.py:61
  94.2 6.2 copy.85
  100.4 54.5 %all-to-all-done = bf16[256,8,896]{2,0,1:T(8,128)(2,1)} async-done(((bf16[256,8,896]{2,0,1:T(8,128)(2,1)}), bf16[256,8,896]{2,0,1:T(8,128)(2,1)}, u32[]{:S(2)}, u32[]{:S(2)}) %all-to-all-start) | async-done | bytes 3670048 | tf_op jit(solution)/shard_map/all_to_all | solution.py:83
  154.8 4.8 all-to-all-start.1
  159.7 3.0 constant_dynamic-slice_fusion.16
  172.2 2.9 collective-permute-start.3
  179.4 13.7 %all-gather.29.cloned.1.call-done = bf16[1,256,7168]{1,2,0:T(8,128)(2,1)} async-done(((bf16[1,256,1792]{1,2,0:T(8,128)(2,1)}), bf16[1,256,7168]{1,2,0:T(8,128)(2,1)}) %all-gather.29.cloned.1.call-update) | async-done | bytes 3670032 | tf_op jit(solution)/shard_map/all_gather | solution.py:62
  193.1 5.2 constant_dynamic-slice_fusion
  201.6 2.0 copy.98
  203.7 2.1 copy.99
  214.0 2.1 copy.105
  220.1 6.6 all-gather.23.cloned.1.call-done
  226.6 6.2 copy.86
  235.3 3.3 collective-permute-start.5
  246.2 46.0 %collective-permute-done.3 = bf16[256,896]{1,0:T(8,128)(2,1)} collective-permute-done((bf16[256,896]{1,0:T(8,128)(2,1)}, bf16[256,896]{1,0:T(8,128)(2,1)}, u32[]{:S(2)}, u32[]{:S(2)}) %collective-permute-start.3) | collective-permute-done | bytes 458784 | tf_op jit(solution)/shard_map/ppermute | solution.py:74
  294.0 8.1 %collective-permute-done.4 = bf16[256,896]{1,0:T(8,128)(2,1)} collective-permute-done((bf16[256,896]{1,0:T(8,128)(2,1)}, bf16[256,896]{1,0:T(8,128)(2,1)}, u32[]{:S(2)}, u32[]{:S(2)}) %collective-permute-start.4) | collective-permute-done | bytes 458784 | tf_op jit(solution)/shard_map/ppermute | solution.py:74
  304.0 7.4 collective-permute-start.10
  312.2 21.2 %collective-permute-start.11 = (bf16[256,896]{1,0:T(8,128)(2,1)}, bf16[256,896]{1,0:T(8,128)(2,1)}, u32[]{:S(2)}, u32[]{:S(2)}) collective-permute-start(bf16[256,896]{1,0:T(8,128)(2,1)} %bitcast.37), channel_id=1, source_target_pairs={{0,10},{2,8},{4,14},{6,12},{8,2},{10,0},{12,6},{14,4},{1,11},{3,9}... | collective-permute-start | bytes 1376264 | tf_op jit(solution)/shard_map/ppermute | solution.py:74
  334.2 5.0 gather_fusion
  339.3 2.3 collective-permute-start.12
  350.1 21.3 %collective-permute-done.10 = bf16[256,896]{1,0:T(8,128)(2,1)} collective-permute-done((bf16[256,896]{1,0:T(8,128)(2,1)}, bf16[256,896]{1,0:T(8,128)(2,1)}, u32[]{:S(2)}, u32[]{:S(2)}) %collective-permute-start.10) | collective-permute-done | bytes 458784 | tf_op jit(solution)/shard_map/ppermute | solution.py:74
  373.2 8.8 %collective-permute-done.11 = bf16[256,896]{1,0:T(8,128)(2,1)} collective-permute-done((bf16[256,896]{1,0:T(8,128)(2,1)}, bf16[256,896]{1,0:T(8,128)(2,1)}, u32[]{:S(2)}, u32[]{:S(2)}) %collective-permute-start.11) | collective-permute-done | bytes 458784 | tf_op jit(solution)/shard_map/ppermute | solution.py:74
  383.8 7.8 collective-permute-start.17
  392.4 21.1 %collective-permute-start.18 = (bf16[256,896]{1,0:T(8,128)(2,1)S(1)}, bf16[256,896]{1,0:T(8,128)(2,1)}, u32[]{:S(2)}, u32[]{:S(2)}) collective-permute-start(bf16[256,896]{1,0:T(8,128)(2,1)S(1)} %bitcast.145), channel_id=1, source_target_pairs={{0,10},{2,8},{4,14},{6,12},{8,2},{10,0},{12,6},{14,4},{1,11},{3,9}... | collective-permute-start | bytes 1376264 | tf_op jit(solution)/shard_map/ppermute | solution.py:74
  414.3 4.8 gather_fusion.1
  428.5 22.5 %collective-permute-done.17 = bf16[256,896]{1,0:T(8,128)(2,1)} collective-permute-done((bf16[256,896]{1,0:T(8,128)(2,1)S(1)}, bf16[256,896]{1,0:T(8,128)(2,1)}, u32[]{:S(2)}, u32[]{:S(2)}) %collective-permute-start.17) | collective-permute-done | bytes 458784 | tf_op jit(solution)/shard_map/ppermute | solution.py:74
  452.9 9.3 %collective-permute-done.18 = bf16[256,896]{1,0:T(8,128)(2,1)} collective-permute-done((bf16[256,896]{1,0:T(8,128)(2,1)S(1)}, bf16[256,896]{1,0:T(8,128)(2,1)}, u32[]{:S(2)}, u32[]{:S(2)}) %collective-permute-start.18) | collective-permute-done | bytes 458784 | tf_op jit(solution)/shard_map/ppermute | solution.py:74
  465.5 4.8 gather_fusion.2
  470.4 18.7 %all-to-all-start.2 = ((bf16[256,8,896]{2,0,1:T(8,128)(2,1)}), bf16[256,8,896]{2,0,1:T(8,128)(2,1)}, u32[]{:S(2)}, u32[]{:S(2)}) async-start(bf16[256,8,896]{2,0,1:T(8,128)(2,1)} %copy.86), calls=%async_computation.2 | async-start | bytes 7340032 | tf_op jit(solution)/shard_map/all_to_all | solution.py:83
  489.7 14.2 %fusion.26 = f32[2048,896]{1,0:T(8,128)} fusion(bf16[2048,896]{1,0:T(8,128)(2,1)} %bitcast.65, bf16[1,2048,2048]{2,1,0:T(8,128)(2,1)} %param.7, f32[2048]{0:T(1024)S(1)} %add_rsqrt_fusion), kind=kOutput, calls=%fused_computation.85 | convolution fusion | flops 7528775680 | bytes 19406848 | tf_op jit(solution)/shard_map/dot_general | solution.py:39
  503.9 14.2 %fusion.22 = f32[2048,896]{1,0:T(8,128)} fusion(bf16[2048,896]{1,0:T(8,128)(2,1)} %bitcast.69, bf16[1,2048,2048]{2,1,0:T(8,128)(2,1)} %param.7, f32[2048]{0:T(1024)S(1)} %add_rsqrt_fusion), kind=kOutput, calls=%fused_computation.84 | convolution fusion | flops 7528775680 | bytes 19406848 | tf_op jit(solution)/shard_map/dot_general | solution.py:39
  518.2 27.0 %fusion.4 = f32[2048,2048]{1,0:T(8,128)} fusion(f32[2048,896]{1,0:T(8,128)} %fusion.26, bf16[2048,896]{1,0:T(8,128)(2,1)} %bitcast.131, bf16[1,896,2048]{2,1,0:T(8,128)(2,1)} %all-gather.31.cloned.1.call-done, bf16[1,2048,2048]{2,1,0:T(8,128)(2,1)} %param.7, f32[2048]{0:T(1024)S(1)} %add_rsqrt_fusion), kind=kOutput, calls=%fused_computation.18 | convolution fusion | flops 15055978496 | bytes 39854080 | tf_op jit(solution)/shard_map/dot_general | solution.py:42
  545.1 26.2 %all-to-all-done.2 = bf16[256,8,896]{2,0,1:T(8,128)(2,1)} async-done(((bf16[256,8,896]{2,0,1:T(8,128)(2,1)}), bf16[256,8,896]{2,0,1:T(8,128)(2,1)}, u32[]{:S(2)}, u32[]{:S(2)}) %all-to-all-start.2) | async-done | bytes 3670048 | tf_op jit(solution)/shard_map/all_to_all | solution.py:83
  571.3 14.2 %fusion.18 = f32[2048,896]{1,0:T(8,128)} fusion(bf16[2048,896]{1,0:T(8,128)(2,1)} %bitcast.73, bf16[1,2048,2048]{2,1,0:T(8,128)(2,1)} %param.7, f32[2048]{0:T(1024)S(1)} %add_rsqrt_fusion), kind=kOutput, calls=%fused_computation.83 | convolution fusion | flops 7528775680 | bytes 19406848 | tf_op jit(solution)/shard_map/dot_general | solution.py:39
  585.6 26.9 %fusion.3 = f32[2048,2048]{1,0:T(8,128)} fusion(f32[2048,896]{1,0:T(8,128)} %fusion.22, bf16[2048,896]{1,0:T(8,128)(2,1)} %bitcast.133, bf16[1,896,2048]{2,1,0:T(8,128)(2,1)} %all-gather.33.cloned.1.call-done, bf16[1,2048,2048]{2,1,0:T(8,128)(2,1)} %param.7, f32[2048]{0:T(1024)S(1)} %add_rsqrt_fusion), kind=kOutput, calls=%fused_computation.17 | convolution fusion | flops 15055978496 | bytes 39854080 | tf_op jit(solution)/shard_map/dot_general | solution.py:42
  612.5 28.7 %add_convert_fusion = bf16[2048,2048]{1,0:T(8,128)(2,1)} fusion(f32[2048,2048]{1,0:T(8,128)} %fusion.3, f32[2048,2048]{1,0:T(8,128)} %fusion.4, f32[2048]{0:T(1024)S(1)} %bitcast.157, f32[2048]{0:T(1024)S(1)} %bitcast.158, f32[2048]{0:T(1024)S(1)} %bitcast.156, f32[2048,896]{1,0:T(8,128)} %fusion.18, bf16[2048,896]{1,0:T(8,128)(2,1)} %bitcast.135, ...), kind=kOutput, calls=%fused_computation.7 | convolution fusion | flops 15081144320 | bytes 65044480 | tf_op jit(solution)/shard_map/dot_general | solution.py:42
  641.2 11.6 %pad_maximum_fusion.2 = bf16[3,896,2048]{2,1,0:T(8,128)(2,1)} fusion(bf16[1,896,2048]{2,1,0:T(8,128)(2,1)} %all-gather.35.cloned.1.call-done, bf16[1,896,2048]{2,1,0:T(8,128)(2,1)} %all-gather.33.cloned.1.call-done, bf16[1,896,2048]{2,1,0:T(8,128)(2,1)} %all-gather.31.cloned.1.call-done), kind=kLoop, calls=%fused_computation.10 | loop fusion | flops 11010048 | bytes 22020096 | tf_op jit(solution)/shard_map/stack | solution.py:94
  652.9 5.0 pad_maximum_fusion.1
  657.9 9.8 %pad_maximum_fusion = bf16[3,2048,896]{2,1,0:T(8,128)(2,1)} fusion(bf16[1,2048,896]{2,1,0:T(8,128)(2,1)} %bitcast.8, bf16[1,2048,896]{2,1,0:T(8,128)(2,1)} %bitcast.5, bf16[1,2048,896]{2,1,0:T(8,128)(2,1)} %bitcast.2), kind=kLoop, calls=%fused_computation.8 | loop fusion | flops 11010048 | bytes 22020096 | tf_op jit(solution)/shard_map/stack | solution.py:92
  667.6 119.3 %reduce-scatter.2.cloned.1.call-done = bf16[256,2048]{1,0:T(8,128)(2,1)} async-done(((bf16[2048,2048]{1,0:T(8,128)(2,1)}), bf16[256,2048]{1,0:T(8,128)(2,1)}) %reduce-scatter.2.cloned.1.call-update) | async-done | bytes 1048592 | tf_op jit(solution)/shard_map/reduce_scatter | solution.py:95
  (132 shorter events, 82.7 us)
Async XLA Ops:
  7.2 53.4 %all-gather.19.cloned.1.call-start = ((), (), s32[]{:S(2)}) async-start(), calls=%async_computation.5 | async-start | bytes 4587520 | tf_op jit(solution)/shard_map/all_gather | solution.py:61
  13.3 6.1 copy-start.10
  26.2 68.0 %all-gather.21.cloned.1.call-start = ((), (), s32[]{:S(2)}) async-start(), calls=%async_computation.6 | async-start | bytes 4587520 | tf_op jit(solution)/shard_map/all_gather | solution.py:61
  26.9 132.7 %all-gather.25.cloned.1.call-start = ((), (), s32[]{:S(2)}) async-start(), calls=%async_computation.8 | async-start | bytes 4587520 | tf_op jit(solution)/shard_map/all_gather | solution.py:62
  28.6 150.8 %all-gather.27.cloned.1.call-start = ((), (), s32[]{:S(2)}) async-start(), calls=%async_computation.9 | async-start | bytes 4587520 | tf_op jit(solution)/shard_map/all_gather | solution.py:62
  29.2 164.0 %all-gather.29.cloned.1.call-start = ((), (), s32[]{:S(2)}) async-start(), calls=%async_computation.10 | async-start | bytes 4587520 | tf_op jit(solution)/shard_map/all_gather | solution.py:62
  29.8 196.9 %all-gather.23.cloned.1.call-start = ((), (), s32[]{:S(2)}) async-start(), calls=%async_computation.7 | async-start | bytes 4587520 | tf_op jit(solution)/shard_map/all_gather | solution.py:61
  30.3 487.8 %all-gather.31.cloned.1.call-start = ((), (), s32[]{:S(2)}) async-start(), calls=%async_computation.11 | async-start | bytes 4587520 | tf_op jit(solution)/shard_map/all_gather | solution.py:63
  34.9 550.6 %all-gather.33.cloned.1.call-start = ((), (), s32[]{:S(2)}) async-start(), calls=%async_computation.12 | async-start | bytes 4587520 | tf_op jit(solution)/shard_map/all_gather | solution.py:63
  66.7 6.4 copy-start.8
  66.7 6.5 copy-start.9
  66.7 88.1 %all-to-all-start = ((bf16[256,8,896]{2,0,1:T(8,128)(2,1)}), bf16[256,8,896]{2,0,1:T(8,128)(2,1)}, u32[]{:S(2)}, u32[]{:S(2)}) async-start(bf16[256,8,896]{2,0,1:T(8,128)(2,1)} %copy.84), calls=%async_computation | async-start | bytes 7340032 | tf_op jit(solution)/shard_map/all_to_all | solution.py:83
  72.4 540.1 %all-gather.35.cloned.1.call-start = ((), (), s32[]{:S(2)}) async-start(), calls=%async_computation.13 | async-start | bytes 4587520 | tf_op jit(solution)/shard_map/all_gather | solution.py:63
  154.8 315.5 %all-to-all-start.1 = ((bf16[256,8,896]{2,0,1:T(8,128)(2,1)}), bf16[256,8,896]{2,0,1:T(8,128)(2,1)}, u32[]{:S(2)}, u32[]{:S(2)}) async-start(bf16[256,8,896]{2,0,1:T(8,128)(2,1)} %copy.85), calls=%async_computation.1 | async-start | bytes 7340032 | tf_op jit(solution)/shard_map/all_to_all | solution.py:83
  165.7 69.6 %collective-permute-start = (bf16[256,896]{1,0:T(8,128)(2,1)}, bf16[256,896]{1,0:T(8,128)(2,1)}, u32[]{:S(2)}, u32[]{:S(2)}) collective-permute-start(bf16[256,896]{1,0:T(8,128)(2,1)} %bitcast.154), channel_id=1, source_target_pairs={{0,2},{2,0},{4,6},{6,4},{8,10},{10,8},{12,14},{14,12},{1,3},{3,1},... | collective-permute-start | bytes 1376264 | tf_op jit(solution)/shard_map/ppermute | solution.py:74
  168.6 71.8 %collective-permute-start.1 = (bf16[256,896]{1,0:T(8,128)(2,1)}, bf16[256,896]{1,0:T(8,128)(2,1)}, u32[]{:S(2)}, u32[]{:S(2)}) collective-permute-start(bf16[256,896]{1,0:T(8,128)(2,1)} %bitcast.13), channel_id=1, source_target_pairs={{0,4},{2,6},{4,0},{6,2},{8,12},{10,14},{12,8},{14,10},{1,5},{3,7},... | collective-permute-start | bytes 1376264 | tf_op jit(solution)/shard_map/ppermute | solution.py:74
  171.1 72.6 %collective-permute-start.2 = (bf16[256,896]{1,0:T(8,128)(2,1)}, bf16[256,896]{1,0:T(8,128)(2,1)}, u32[]{:S(2)}, u32[]{:S(2)}) collective-permute-start(bf16[256,896]{1,0:T(8,128)(2,1)} %bitcast.15), channel_id=1, source_target_pairs={{0,6},{2,4},{4,2},{6,0},{8,14},{10,12},{12,10},{14,8},{1,7},{3,5},... | collective-permute-start | bytes 1376264 | tf_op jit(solution)/shard_map/ppermute | solution.py:74
  172.2 120.0 %collective-permute-start.3 = (bf16[256,896]{1,0:T(8,128)(2,1)}, bf16[256,896]{1,0:T(8,128)(2,1)}, u32[]{:S(2)}, u32[]{:S(2)}) collective-permute-start(bf16[256,896]{1,0:T(8,128)(2,1)} %bitcast.17), channel_id=1, source_target_pairs={{0,8},{2,10},{4,12},{6,14},{8,0},{10,2},{12,4},{14,6},{1,9},{3,11}... | collective-permute-start | bytes 1376264 | tf_op jit(solution)/shard_map/ppermute | solution.py:74
  176.0 126.1 %collective-permute-start.4 = (bf16[256,896]{1,0:T(8,128)(2,1)}, bf16[256,896]{1,0:T(8,128)(2,1)}, u32[]{:S(2)}, u32[]{:S(2)}) collective-permute-start(bf16[256,896]{1,0:T(8,128)(2,1)} %bitcast.19), channel_id=1, source_target_pairs={{0,10},{2,8},{4,14},{6,12},{8,2},{10,0},{12,6},{14,4},{1,11},{3,9}... | collective-permute-start | bytes 1376264 | tf_op jit(solution)/shard_map/ppermute | solution.py:74
  226.6 6.3 copy-start.3
  232.9 7.6 copy-start.7
  235.3 68.7 %collective-permute-start.5 = (bf16[256,896]{1,0:T(8,128)(2,1)}, bf16[256,896]{1,0:T(8,128)(2,1)S(1)}, u32[]{:S(2)}, u32[]{:S(2)}) collective-permute-start(bf16[256,896]{1,0:T(8,128)(2,1)} %bitcast.153), channel_id=1, source_target_pairs={{0,12},{2,14},{4,8},{6,10},{8,4},{10,6},{12,0},{14,2},{1,13},{3,15... | collective-permute-start | bytes 1376264 | tf_op jit(solution)/shard_map/ppermute | solution.py:74
  240.5 71.7 %collective-permute-start.6 = (bf16[256,896]{1,0:T(8,128)(2,1)S(1)}, bf16[256,896]{1,0:T(8,128)(2,1)S(1)}, u32[]{:S(2)}, u32[]{:S(2)}) collective-permute-start(bf16[256,896]{1,0:T(8,128)(2,1)S(1)} %bitcast.152), channel_id=1, source_target_pairs={{0,14},{2,12},{4,10},{6,8},{8,6},{10,4},{12,2},{14,0},{1,15},{3,13... | collective-permute-start | bytes 1376264 | tf_op jit(solution)/shard_map/ppermute | solution.py:74
  243.8 95.5 %collective-permute-start.7 = (bf16[256,896]{1,0:T(8,128)(2,1)}, bf16[256,896]{1,0:T(8,128)(2,1)}, u32[]{:S(2)}, u32[]{:S(2)}) collective-permute-start(bf16[256,896]{1,0:T(8,128)(2,1)} %bitcast.29), channel_id=1, source_target_pairs={{0,2},{2,0},{4,6},{6,4},{8,10},{10,8},{12,14},{14,12},{1,3},{3,1},... | collective-permute-start | bytes 1376264 | tf_op jit(solution)/shard_map/ppermute | solution.py:74
  292.2 51.2 %collective-permute-start.8 = (bf16[256,896]{1,0:T(8,128)(2,1)}, bf16[256,896]{1,0:T(8,128)(2,1)}, u32[]{:S(2)}, u32[]{:S(2)}) collective-permute-start(bf16[256,896]{1,0:T(8,128)(2,1)} %bitcast.31), channel_id=1, source_target_pairs={{0,4},{2,6},{4,0},{6,2},{8,12},{10,14},{12,8},{14,10},{1,5},{3,7},... | collective-permute-start | bytes 1376264 | tf_op jit(solution)/shard_map/ppermute | solution.py:74
  302.2 44.7 %collective-permute-start.9 = (bf16[256,896]{1,0:T(8,128)(2,1)}, bf16[256,896]{1,0:T(8,128)(2,1)}, u32[]{:S(2)}, u32[]{:S(2)}) collective-permute-start(bf16[256,896]{1,0:T(8,128)(2,1)} %bitcast.33), channel_id=1, source_target_pairs={{0,6},{2,4},{4,2},{6,0},{8,14},{10,12},{12,10},{14,8},{1,7},{3,5},... | collective-permute-start | bytes 1376264 | tf_op jit(solution)/shard_map/ppermute | solution.py:74
  304.0 67.4 %collective-permute-start.10 = (bf16[256,896]{1,0:T(8,128)(2,1)}, bf16[256,896]{1,0:T(8,128)(2,1)}, u32[]{:S(2)}, u32[]{:S(2)}) collective-permute-start(bf16[256,896]{1,0:T(8,128)(2,1)} %bitcast.35), channel_id=1, source_target_pairs={{0,8},{2,10},{4,12},{6,14},{8,0},{10,2},{12,4},{14,6},{1,9},{3,11}... | collective-permute-start | bytes 1376264 | tf_op jit(solution)/shard_map/ppermute | solution.py:74
  312.2 69.8 %collective-permute-start.11 = (bf16[256,896]{1,0:T(8,128)(2,1)}, bf16[256,896]{1,0:T(8,128)(2,1)}, u32[]{:S(2)}, u32[]{:S(2)}) collective-permute-start(bf16[256,896]{1,0:T(8,128)(2,1)} %bitcast.37), channel_id=1, source_target_pairs={{0,10},{2,8},{4,14},{6,12},{8,2},{10,0},{12,6},{14,4},{1,11},{3,9}... | collective-permute-start | bytes 1376264 | tf_op jit(solution)/shard_map/ppermute | solution.py:74
  334.2 12.6 %copy-start.6 = (bf16[256,1,896]{2,0,1:T(8,128)(2,1)S(1)}, bf16[256,1,896]{2,0,1:T(8,128)(2,1)}, u32[]{:S(2)}) copy-start(bf16[256,1,896]{2,0,1:T(8,128)(2,1)} %copy.105) | copy-start | bytes 1376260
  334.2 37.1 %copy-start.5 = (bf16[256,1,896]{2,0,1:T(8,128)(2,1)S(1)}, bf16[256,1,896]{2,0,1:T(8,128)(2,1)}, u32[]{:S(2)}) copy-start(bf16[256,1,896]{2,0,1:T(8,128)(2,1)} %copy.106) | copy-start | bytes 1376260
  339.3 42.7 %copy-start.4 = (bf16[256,1,896]{2,0,1:T(8,128)(2,1)S(1)}, bf16[256,1,896]{2,0,1:T(8,128)(2,1)}, u32[]{:S(2)}) copy-start(bf16[256,1,896]{2,0,1:T(8,128)(2,1)} %copy.107) | copy-start | bytes 1376260
  339.3 44.5 %collective-permute-start.12 = (bf16[256,896]{1,0:T(8,128)(2,1)}, bf16[256,896]{1,0:T(8,128)(2,1)S(1)}, u32[]{:S(2)}, u32[]{:S(2)}) collective-permute-start(bf16[256,896]{1,0:T(8,128)(2,1)} %bitcast.151), channel_id=1, source_target_pairs={{0,12},{2,14},{4,8},{6,10},{8,4},{10,6},{12,0},{14,2},{1,13},{3,15... | collective-permute-start | bytes 1376264 | tf_op jit(solution)/shard_map/ppermute | solution.py:74
  343.3 49.0 %collective-permute-start.13 = (bf16[256,896]{1,0:T(8,128)(2,1)}, bf16[256,896]{1,0:T(8,128)(2,1)S(1)}, u32[]{:S(2)}, u32[]{:S(2)}) collective-permute-start(bf16[256,896]{1,0:T(8,128)(2,1)} %bitcast.150), channel_id=1, source_target_pairs={{0,14},{2,12},{4,10},{6,8},{8,6},{10,4},{12,2},{14,0},{1,15},{3,13... | collective-permute-start | bytes 1376264 | tf_op jit(solution)/shard_map/ppermute | solution.py:74
  346.9 72.3 %collective-permute-start.14 = (bf16[256,896]{1,0:T(8,128)(2,1)S(1)}, bf16[256,896]{1,0:T(8,128)(2,1)}, u32[]{:S(2)}, u32[]{:S(2)}) collective-permute-start(bf16[256,896]{1,0:T(8,128)(2,1)S(1)} %bitcast.149), channel_id=1, source_target_pairs={{0,2},{2,0},{4,6},{6,4},{8,10},{10,8},{12,14},{14,12},{1,3},{3,1},... | collective-permute-start | bytes 1376264 | tf_op jit(solution)/shard_map/ppermute | solution.py:74
  371.4 51.6 %collective-permute-start.15 = (bf16[256,896]{1,0:T(8,128)(2,1)S(1)}, bf16[256,896]{1,0:T(8,128)(2,1)}, u32[]{:S(2)}, u32[]{:S(2)}) collective-permute-start(bf16[256,896]{1,0:T(8,128)(2,1)S(1)} %bitcast.148), channel_id=1, source_target_pairs={{0,4},{2,6},{4,0},{6,2},{8,12},{10,14},{12,8},{14,10},{1,5},{3,7},... | collective-permute-start | bytes 1376264 | tf_op jit(solution)/shard_map/ppermute | solution.py:74
  382.0 44.7 %collective-permute-start.16 = (bf16[256,896]{1,0:T(8,128)(2,1)S(1)}, bf16[256,896]{1,0:T(8,128)(2,1)}, u32[]{:S(2)}, u32[]{:S(2)}) collective-permute-start(bf16[256,896]{1,0:T(8,128)(2,1)S(1)} %bitcast.147), channel_id=1, source_target_pairs={{0,6},{2,4},{4,2},{6,0},{8,14},{10,12},{12,10},{14,8},{1,7},{3,5},... | collective-permute-start | bytes 1376264 | tf_op jit(solution)/shard_map/ppermute | solution.py:74
  383.8 67.2 %collective-permute-start.17 = (bf16[256,896]{1,0:T(8,128)(2,1)S(1)}, bf16[256,896]{1,0:T(8,128)(2,1)}, u32[]{:S(2)}, u32[]{:S(2)}) collective-permute-start(bf16[256,896]{1,0:T(8,128)(2,1)S(1)} %bitcast.146), channel_id=1, source_target_pairs={{0,8},{2,10},{4,12},{6,14},{8,0},{10,2},{12,4},{14,6},{1,9},{3,11}... | collective-permute-start | bytes 1376264 | tf_op jit(solution)/shard_map/ppermute | solution.py:74
  392.4 69.7 %collective-permute-start.18 = (bf16[256,896]{1,0:T(8,128)(2,1)S(1)}, bf16[256,896]{1,0:T(8,128)(2,1)}, u32[]{:S(2)}, u32[]{:S(2)}) collective-permute-start(bf16[256,896]{1,0:T(8,128)(2,1)S(1)} %bitcast.145), channel_id=1, source_target_pairs={{0,10},{2,8},{4,14},{6,12},{8,2},{10,0},{12,6},{14,4},{1,11},{3,9}... | collective-permute-start | bytes 1376264 | tf_op jit(solution)/shard_map/ppermute | solution.py:74
  419.1 44.8 %collective-permute-start.19 = (bf16[256,896]{1,0:T(8,128)(2,1)S(1)}, bf16[256,896]{1,0:T(8,128)(2,1)S(1)}, u32[]{:S(2)}, u32[]{:S(2)}) collective-permute-start(bf16[256,896]{1,0:T(8,128)(2,1)S(1)} %bitcast.144), channel_id=1, source_target_pairs={{0,12},{2,14},{4,8},{6,10},{8,4},{10,6},{12,0},{14,2},{1,13},{3,15... | collective-permute-start | bytes 1376264 | tf_op jit(solution)/shard_map/ppermute | solution.py:74
  422.9 41.8 %collective-permute-start.20 = (bf16[256,896]{1,0:T(8,128)(2,1)S(1)}, bf16[256,896]{1,0:T(8,128)(2,1)S(1)}, u32[]{:S(2)}, u32[]{:S(2)}) collective-permute-start(bf16[256,896]{1,0:T(8,128)(2,1)S(1)} %bitcast.143), channel_id=1, source_target_pairs={{0,14},{2,12},{4,10},{6,8},{8,6},{10,4},{12,2},{14,0},{1,15},{3,13... | collective-permute-start | bytes 1376264 | tf_op jit(solution)/shard_map/ppermute | solution.py:74
  470.4 101.0 %all-to-all-start.2 = ((bf16[256,8,896]{2,0,1:T(8,128)(2,1)}), bf16[256,8,896]{2,0,1:T(8,128)(2,1)}, u32[]{:S(2)}, u32[]{:S(2)}) async-start(bf16[256,8,896]{2,0,1:T(8,128)(2,1)} %copy.86), calls=%async_computation.2 | async-start | bytes 7340032 | tf_op jit(solution)/shard_map/all_to_all | solution.py:83
  489.1 297.8 %reduce-scatter.2.cloned.1.call-start = ((), (), s32[]{:S(2)}) async-start(), calls=%async_computation.4 | async-start | bytes 9437184 | tf_op jit(solution)/shard_map/reduce_scatter | solution.py:95
  641.2 11.6 %copy-start = (bf16[8,256,896]{2,1,0:T(8,128)(2,1)S(1)}, bf16[8,256,896]{2,1,0:T(8,128)(2,1)}, u32[]{:S(2)}) copy-start(bf16[8,256,896]{2,1,0:T(8,128)(2,1)} %gather_fusion) | copy-start | bytes 11010052
  641.2 11.6 %copy-start.1 = (bf16[8,256,896]{2,1,0:T(8,128)(2,1)S(1)}, bf16[8,256,896]{2,1,0:T(8,128)(2,1)}, u32[]{:S(2)}) copy-start(bf16[8,256,896]{2,1,0:T(8,128)(2,1)} %gather_fusion.1) | copy-start | bytes 11010052
  641.2 11.6 %copy-start.2 = (bf16[8,256,896]{2,1,0:T(8,128)(2,1)S(1)}, bf16[8,256,896]{2,1,0:T(8,128)(2,1)}, u32[]{:S(2)}) copy-start(bf16[8,256,896]{2,1,0:T(8,128)(2,1)} %gather_fusion.2) | copy-start | bytes 11010052
Sparse Core Ops, SparseCore 0:
  26.3 34.1 all-gather.18
  62.7 31.4 all-gather.20
  95.8 31.4 all-gather.24
  128.7 31.4 all-gather.26
  161.6 31.4 all-gather.28
  195.1 31.4 all-gather.22
  228.2 31.4 all-gather.30
  261.3 31.4 all-gather.32
  294.4 31.4 all-gather.34
  641.3 145.5 reduce-scatter.1
